TPU v7x, 32 devices: a whole 2x2x4 slice. The times are simulated.
32 devices in a mesh: grp: 2 (over x), ep: 16 (over z, y, core).
Axes of the slice: x: 2, y: 2, z: 4, core: 2. Of those that a mesh axis runs over, the one named last changes fastest.
Arguments:
- tokens: bfloat16 [8192, 2048], P(('grp', 'ep')), parts along dimension 0, may hold values from -6 to 6
- norm_gain: float32 [2048], replicated, may hold values from 0.1 to 1.9
- route_ids: int32 [8192, 2], P(('grp', 'ep')), parts along dimension 0, may hold values from 0 to 15, as said below
- route_slots: int32 [8192, 2], P(('grp', 'ep')), parts along dimension 0, may hold values from 0 to 47, as said below
- route_weights: float32 [8192, 2], P(('grp', 'ep')), parts along dimension 0, may hold values from 0.1 to 1
- w_gate: bfloat16 [16, 2048, 512], P('ep'), may hold values from -0.125 to 0.125
- w_up: bfloat16 [16, 2048, 512], P('ep'), may hold values from -0.125 to 0.125
- w_down: bfloat16 [16, 512, 2048], P('ep'), may hold values from -0.25 to 0.25
Outputs:
- expert_mix: bfloat16 [8192, 2048], P(('grp', 'ep')), parts along dimension 0
There are 2 independent parts, one for each index of `grp`. A program takes and returns all parts, laid end to end along the dimension named above; an argument that names none is the same for every part. Nothing has to cross between parts.
Inputs may be any that keep to these rules, and one draw needn't show every extreme that they name: `route_ids`: expert e belongs to group e // 4. Each token names 2 different experts of one group. In each aligned block of 256 tokens (the rows of one device) no expert is named more than 48 times, and some expert exactly 48 times. `route_slots`: in each aligned block of 256 tokens, the entries that name one expert hold distinct slots 0, 1, ... up to their count less one.
All inputs are finite; a program needn't handle non-finite values.
Results may differ from a plain program's by a relative error of at most 0.007.
Values may be sent and summed in bfloat16 or wider, within the bound.
A program may use at most 64 MiB of HBM per device.

v0:
```python
import jax
import jax.numpy as jnp
from jax import lax
from jax.sharding import PartitionSpec as P


def shards(tokens, norm_gain, route_ids, route_slots, route_weights, w_gate, w_up, w_down):
    tok_rows = tokens.shape[0]
    feat_dim = tokens.shape[1]
    n_devices = lax.axis_size("ep")
    local_count = w_gate.shape[0]
    experts_all = n_devices * local_count
    top_count = route_ids.shape[1]
    capacity = 3 * top_count * tok_rows // (2 * experts_all)
    tok_f32 = tokens.astype(jnp.float32)
    scale = lax.rsqrt(jnp.mean(tok_f32 * tok_f32, axis=-1, keepdims=True) + 1e-06)
    normed = (tok_f32 * scale * norm_gain).astype(jnp.bfloat16)
    place_idx = (route_ids * capacity + route_slots).reshape(-1)
    send = jnp.zeros((experts_all * capacity, feat_dim), jnp.bfloat16)
    send = send.at[place_idx].set(jnp.repeat(normed, top_count, axis=0))
    send = send.reshape(n_devices, local_count, capacity, feat_dim)
    rows_in = lax.all_to_all(send, "ep", split_axis=0, concat_axis=0, tiled=True)
    gate_act = jnp.einsum("sxcd,xdf->sxcf", rows_in, w_gate, preferred_element_type=jnp.float32)
    up_act = jnp.einsum("sxcd,xdf->sxcf", rows_in, w_up, preferred_element_type=jnp.float32)
    hidden = (jax.nn.silu(gate_act) * up_act).astype(jnp.bfloat16)
    results = jnp.einsum(
        "sxcf,xfd->sxcd", hidden, w_down, preferred_element_type=jnp.float32
    ).astype(jnp.bfloat16)
    returned = lax.all_to_all(results, "ep", split_axis=0, concat_axis=0, tiled=True)
    flat_rows = returned.reshape(experts_all * capacity, feat_dim)
    picked = flat_rows[place_idx].reshape(tok_rows, top_count, feat_dim).astype(jnp.float32)
    mixed = jnp.sum(route_weights[:, :, None] * picked, axis=1)
    return mixed.astype(jnp.bfloat16)


def solution(mesh):
    placed = (
        P(("grp", "ep"), None),
        P(),
        P(("grp", "ep"), None),
        P(("grp", "ep"), None),
        P(("grp", "ep"), None),
        P("ep", None, None),
        P("ep", None, None),
        P("ep", None, None),
    )
    return jax.shard_map(
        shards, mesh=mesh, in_specs=placed, out_specs=P(("grp", "ep"), None), check_vma=False
    )
```

profile of v0, /device:TPU:15, one launch (start us, length us, event | category | flops | bytes accessed | tf_op | source)
XLA Modules:
  0.0 205.0 jit_solution(18275596200119128683)
XLA Ops:
  0.0 0.0 copy-start
  0.0 0.9 multiply_add_fusion
  0.9 0.1 copy.13
  1.0 0.1 reshape.73
  1.2 1.5 fusion.5
  2.7 1.5 fusion.7
  4.2 2.6 %broadcast_in_dim.5 = bf16[256,2,2048]{2,1,0:T(2,128)(2,1)} broadcast(bf16[256,2048]{1,0:T(8,128)(2,1)S(1)} %fusion.7), dimensions={0,2} | broadcast | bytes 3145728 | tf_op jit(solution)/shard_map/broadcast_in_dim | solution.py:20
  6.8 4.1 %reshape.95 = bf16[512,2048]{1,0:T(8,128)(2,1)} reshape(bf16[256,2,2048]{2,1,0:T(2,128)(2,1)} %broadcast_in_dim.5) | data formatting | bytes 4194304 | tf_op jit(solution)/shard_map/reshape | solution.py:20
  10.9 6.7 %scatter_custom_fusion = bf16[768,2048]{1,0:T(8,128)(2,1)} fusion(s32[512]{0:T(512)S(1)} %bitcast.78, bf16[512,2048]{1,0:T(8,128)(2,1)} %reshape.95, bf16[]{:T(256)} %constant.2.clone.1), kind=kCustom, calls=%fused_computation.24 | custom fusion | bytes 3146240 | tf_op jit(solution)/shard_map/scatter | solution.py:20
  17.6 0.0 copy-start.3
  17.6 76.4 %all_to_all.10 = bf16[16,1,48,2048]{3,2,1,0:T(8,128)(2,1)S(1)} all-to-all(bf16[16,1,48,2048]{3,2,1,0:T(8,128)(2,1)} %bitcast.77), channel_id=1, replica_groups=mesh['grp'=2,'ep'=16] {'ep'}, dimensions={0} | all-to-all | bytes 6291456 | tf_op jit(solution)/shard_map/all_to_all | solution.py:22
  94.0 0.0 copy-start.1
  94.0 1.7 copy-done.1
  95.7 0.0 copy-done.3
  95.7 2.9 %fusion.2 = f32[16,48,512]{2,1,0:T(8,128)} fusion(bf16[16,1,48,2048]{3,2,1,0:T(8,128)(2,1)S(1)} %all_to_all.10, bf16[1,2048,512]{2,1,0:T(8,128)(2,1)S(1)} %copy-done.3), kind=kOutput, calls=%fused_computation.6 | convolution fusion | flops 1610612736 | bytes 6815744 | tf_op jit(solution)/shard_map/sxcd,xdf->sxcf/dot_general | solution.py:23
  98.7 0.0 copy-done
  98.7 8.1 %fusion.4 = bf16[16,1,48,2048]{3,2,1,0:T(8,128)(2,1)} fusion(bf16[1,512,2048]{2,1,0:T(8,128)(2,1)S(1)} %copy-done, bf16[1,2048,512]{2,1,0:T(8,128)(2,1)} %param.14, bf16[16,1,48,2048]{3,2,1,0:T(8,128)(2,1)} %copy-done.1, f32[16,48,512]{2,1,0:T(8,128)} %fusion.2), kind=kOutput, calls=%fused_computation.8 | convolution fusion | flops 3225157632 | bytes 12058624 | tf_op jit(solution)/shard_map/sxcf,xfd->sxcd/dot_general | solution.py:26
  106.8 0.0 copy-start.2
  106.8 5.2 %all-to-all-start.1 = ((bf16[16,1,48,2048]{3,2,1,0:T(8,128)(2,1)}), bf16[16,1,48,2048]{3,2,1,0:T(8,128)(2,1)}, u32[]{:S(2)}, u32[]{:S(2)}) async-start(bf16[16,1,48,2048]{3,2,1,0:T(8,128)(2,1)} %fusion.4), calls=%async_computation.1 | async-start | bytes 6291456 | tf_op jit(solution)/shard_map/all_to_all | solution.py:29
  112.1 0.0 copy-done.2
  112.1 0.1 copy.12
  112.2 69.8 %all-to-all-done.1 = bf16[16,1,48,2048]{3,2,1,0:T(8,128)(2,1)} async-done(((bf16[16,1,48,2048]{3,2,1,0:T(8,128)(2,1)}), bf16[16,1,48,2048]{3,2,1,0:T(8,128)(2,1)}, u32[]{:S(2)}, u32[]{:S(2)}) %all-to-all-start.1) | async-done | bytes 3145760 | tf_op jit(solution)/shard_map/all_to_all | solution.py:29
  182.0 7.6 %gather_fusion = bf16[512,2048]{1,0:T(8,128)(2,1)} fusion(bf16[768,2048]{1,0:T(8,128)(2,1)} %bitcast.22, s32[1024]{0:T(1024)S(1)} %pad_clamp_fusion), kind=kCustom, calls=%fused_computation | custom fusion | bytes 4196352 | tf_op jit(solution)/shard_map/gather | solution.py:31
  189.6 5.5 %reshape.82 = f32[256,2,2048]{2,1,0:T(2,128)} reshape(bf16[512,2048]{1,0:T(8,128)(2,1)} %gather_fusion) | data formatting | bytes 6291456 | tf_op jit(solution)/shard_map/convert_element_type | solution.py:31
  195.1 9.9 %multiply_reduce_fusion = bf16[256,2048]{1,0:T(8,128)(2,1)} fusion(f32[256,2,2048]{2,1,0:T(2,128)} %reshape.82, f32[256,2]{1,0:T(8,128)S(1)} %copy.12), kind=kLoop, calls=%fused_computation.2 | loop fusion | flops 1572864 | bytes 5244928 | tf_op jit(solution)/shard_map/reduce_sum | solution.py:32
  (3 shorter events, 0.0 us)
Async XLA Ops:
  0.0 98.7 %copy-start = (bf16[1,512,2048]{2,1,0:T(8,128)(2,1)S(1)}, bf16[1,512,2048]{2,1,0:T(8,128)(2,1)}, u32[]{:S(2)}) copy-start(bf16[1,512,2048]{2,1,0:T(8,128)(2,1)} %param.15) | copy-start | bytes 6291460
  17.6 78.1 %copy-start.3 = (bf16[1,2048,512]{2,1,0:T(8,128)(2,1)S(1)}, bf16[1,2048,512]{2,1,0:T(8,128)(2,1)}, u32[]{:S(2)}) copy-start(bf16[1,2048,512]{2,1,0:T(8,128)(2,1)} %param.13) | copy-start | bytes 6291460
  94.0 1.7 copy-start.1
  106.8 5.2 %copy-start.2 = (f32[256,2]{0,1:T(2,128)S(1)}, f32[256,2]{0,1:T(2,128)}, u32[]{:S(2)}) copy-start(f32[256,2]{0,1:T(2,128)} %param.12) | copy-start | bytes 6148
  106.8 75.2 %all-to-all-start.1 = ((bf16[16,1,48,2048]{3,2,1,0:T(8,128)(2,1)}), bf16[16,1,48,2048]{3,2,1,0:T(8,128)(2,1)}, u32[]{:S(2)}, u32[]{:S(2)}) async-start(bf16[16,1,48,2048]{3,2,1,0:T(8,128)(2,1)} %fusion.4), calls=%async_computation.1 | async-start | bytes 6291456 | tf_op jit(solution)/shard_map/all_to_all | solution.py:29
where the time goes:
time: 206 us; the launch traced here: 205 us
  blocking collectives  76.4 us (37%)
  waiting for transfers between devices  69.8 us (34%)
  local copies, waits for them, and re-layouts  28.6 us (14%)
  other arithmetic  13.8 us (7%)
  matrix products  11.1 us (5%)
  starting transfers between devices  5.24 us (3%)
    all_to_all x1, blocking collectives, shards(): lax.all_to_all(send, 'ep', split_axis=0, concat_axis=0, tiled=True)  76.4 us
    all_to_all x1, waiting for transfers between devices, shards(): lax.all_to_all(results, 'ep', split_axis=0, concat_axis=0, tiled=True)  69.8 us
    reduce_sum x1, other arithmetic, shards(): mixed = jnp.sum(route_weights[:, :, None] * picked, axis=1)  9.86 us
    dot_general x1, matrix products, shards(): jnp.einsum('sxcf,xfd->sxcd', hidden, w_down, preferred_element_type=jnp.f...  8.14 us
    gather x1, local copies, waits for them, and re-layouts, shards(): flat_rows[place_idx].reshape(tok_rows, top_count, feat_dim)  7.58 us
    scatter x1, local copies, waits for them, and re-layouts, shards(): send = send.at[place_idx].set(jnp.repeat(normed, top_count, axis=0))  6.73 us
    convert_element_type x1, local copies, waits for them, and re-layouts, shards(): flat_rows[place_idx].reshape(tok_rows, top_count, feat_dim)  5.48 us
    all_to_all x1, starting transfers between devices, shards(): lax.all_to_all(results, 'ep', split_axis=0, concat_axis=0, tiled=True)  5.24 us
  transfers between devices with their start and end apart: 1, of which 1 were waited for; matrix products, arithmetic and copies ran while one was open for 0% of the time, Pallas kernels for 0%

commit v1 on v0

v1 whole, which is shorter than its diff:
```python
import functools

import jax
import jax.numpy as jnp
from jax import lax
from jax.experimental import pallas as pl
from jax.experimental.pallas import tpu as pltpu
from jax.sharding import PartitionSpec as P

GROUPS = 4
META = 128
ORDER = (2, 1, 3)
NT = (((1,), (1,)), ((), ()))
F32 = jnp.float32
BF16 = jnp.bfloat16


def flip(index, bits):
    out, weight = index, 1
    while weight <= bits:
        if bits & weight:
            out = out + weight * (1 - 2 * ((index // weight) % 2))
        weight *= 2
    return out


def kernel(
    peers, cap, capp,
    tok, gain, ids, slots, wts, wg_hbm, wu_hbm, wd_hbm,
    out,
    normed, x_out, x_in, y_out, e_in, hid, r_out, r_in, m_out, h_in, wg, wu, wd,
    w_sem, xs, xr, ys, yr, rs, rr, hs, hr,
):
    rows, feat = tok.shape
    ffn = wg.shape[1]
    block = x_out.shape[1]
    spread = peers * capp
    me = lax.axis_index("ep")
    group, rank = me // peers, me % peers
    shift = peers.bit_length() - 1

    def at(d, j):
        return {"ep": flip(group, d) * peers + flip(rank, j)}

    barrier = pltpu.get_barrier_semaphore()
    for d in range(1, GROUPS):
        pl.semaphore_signal(barrier, inc=1, device_id=at(d, 0), device_id_type=pl.DeviceIdType.MESH)
    for j in range(1, peers):
        pl.semaphore_signal(barrier, inc=1, device_id=at(0, j), device_id_type=pl.DeviceIdType.MESH)

    loads = [
        pltpu.make_async_copy(src, dst, w_sem.at[i])
        for i, (src, dst) in enumerate(((wg_hbm, wg), (wu_hbm, wu), (wd_hbm, wd)))
    ]
    for load in loads:
        load.start()

    def remote(src, dst, send, recv, where):
        return pltpu.make_async_remote_copy(
            src_ref=src, dst_ref=dst, send_sem=send, recv_sem=recv,
            device_id=where, device_id_type=pl.DeviceIdType.MESH,
        )

    step = 32

    def norm_rows(i, carry):
        at_rows = pl.ds(i * step, step)
        v = tok[at_rows, :].astype(F32)
        scale = lax.rsqrt(jnp.mean(v * v, axis=-1, keepdims=True) + 1e-06)
        normed[at_rows, :feat] = (v * scale * gain[...]).astype(BF16)
        return carry

    lax.fori_loop(0, rows // step, norm_rows, 0)

    lane = lax.broadcasted_iota(jnp.int32, (rows, META), 1)
    meta = jnp.zeros((rows, META), F32)
    for k in range(2):
        e = ids[:, k:k + 1]
        code = (((e & (peers - 1)) ^ rank) * capp + slots[:, k:k + 1] + 1).astype(F32)
        meta = jnp.where(lane == k, code, meta)
        w = wts[:, k:k + 1]
        for part in range(3):
            piece = w.astype(BF16).astype(F32)
            meta = jnp.where(lane == 2 + 3 * k + part, piece, meta)
            w = w - piece
    normed[:, feat:] = meta.astype(BF16)

    tok_group = ids[:, 0:1] >> shift
    member = jnp.where(lane == tok_group, 1.0, 0.0)
    earlier = jnp.where(
        lax.broadcasted_iota(jnp.int32, (rows, rows), 1) < lax.broadcasted_iota(jnp.int32, (rows, rows), 0),
        1.0, 0.0,
    ).astype(BF16)
    before = jnp.dot(earlier, member.astype(BF16), preferred_element_type=F32)
    place = jnp.sum(before * member, axis=1, keepdims=True)
    facts = jnp.where(lane == 0, tok_group.astype(F32), jnp.where(lane == 1, place, 0.0))
    pick16 = jnp.where(
        lax.broadcasted_iota(jnp.int32, (16, META), 0) == lax.broadcasted_iota(jnp.int32, (16, META), 1),
        1.0, 0.0,
    ).astype(BF16)
    across = lax.dot_general(pick16, facts.astype(BF16), NT, preferred_element_type=F32)
    group_row, place_row = across[0:1, :], across[1:2, :]
    row_no = lax.broadcasted_iota(jnp.int32, (block, rows), 0).astype(F32)
    tile = 512

    def pack(d):
        hit = (row_no == place_row) & (group_row == flip(group, d).astype(F32))
        pick = jnp.where(hit, 1.0, 0.0).astype(BF16)

        def cols(i, carry):
            c = pl.ds(pl.multiple_of(i * tile, tile), tile)
            x_out[d, :, c] = jnp.dot(pick, normed[:, c], preferred_element_type=F32).astype(BF16)
            return carry

        lax.fori_loop(0, feat // tile, cols, 0)
        x_out[d, :, feat:] = jnp.dot(pick, normed[:, feat:], preferred_element_type=F32).astype(BF16)

    x_copies = {}
    for n, d in enumerate(ORDER):
        pack(d)
        if n == 0:
            pl.semaphore_wait(barrier, GROUPS - 1 + peers - 1)
        x_copies[d] = remote(x_out.at[d], x_in.at[d], xs.at[d], xr.at[d], at(d, 0))
        x_copies[d].start()
    pack(0)

    y_copies, r_copies, h_copies = {}, {}, {}

    def chunk(j):
        return pl.ds(j * capp, capp)

    def dispatch(d):
        src = x_out if d == 0 else x_in
        if d:
            x_copies[d].wait_recv()
        codes = lax.dot_general(pick16, src[d, :, feat:], NT, preferred_element_type=F32)
        slot = (lax.broadcasted_iota(jnp.int32, (spread, block), 0) + 1).astype(F32)
        hit = (slot == codes[0:1, :]) | (slot == codes[1:2, :])
        pick = jnp.where(hit, 1.0, 0.0).astype(BF16)

        def cols(i, carry):
            c = pl.ds(pl.multiple_of(i * tile, tile), tile)
            got = jnp.dot(pick, src[d, :, c], preferred_element_type=F32).astype(BF16)
            e_in[d, :capp, c] = got[:capp]
            y_out[d, capp:, c] = got[capp:]
            return carry

        lax.fori_loop(0, feat // tile, cols, 0)
        for j in range(1, peers):
            copy = remote(y_out.at[d, chunk(j)], e_in.at[d, chunk(j)], ys.at[d, j], yr.at[d, j], at(0, j))
            copy.start()
            y_copies[d, j] = copy

    def compute(d):
        if not r_copies:
            for load in loads:
                load.wait()
        for j in range(1, peers):
            y_copies[d, j].wait_recv()
        half = 256

        def up(i, carry):
            c = pl.ds(pl.multiple_of(i * half, half), half)
            gate = jnp.dot(e_in[d], wg[:, c], preferred_element_type=F32)
            upper = jnp.dot(e_in[d], wu[:, c], preferred_element_type=F32)
            hid[:, c] = (gate / (1.0 + jnp.exp(-gate)) * upper).astype(BF16)
            return carry

        lax.fori_loop(0, ffn // half, up, 0)

        def down(i, carry):
            c = pl.ds(pl.multiple_of(i * tile, tile), tile)
            got = jnp.dot(hid[...], wd[:, c], preferred_element_type=F32).astype(BF16)
            r_in[d, :capp, c] = got[:capp]
            r_out[d, capp:, c] = got[capp:]
            return carry

        lax.fori_loop(0, feat // tile, down, 0)
        for j in range(1, peers):
            copy = remote(r_out.at[d, chunk(j)], r_in.at[d, chunk(j)], rs.at[d, j], rr.at[d, j], at(0, j))
            copy.start()
            r_copies[d, j] = copy

    def combine(d):
        src = x_out if d == 0 else x_in
        for j in range(1, peers):
            r_copies[d, j].wait_recv()
        info = src[d, :, feat:].astype(F32)
        slot = (lax.broadcasted_iota(jnp.int32, (block, spread), 1) + 1).astype(F32)
        picks = [jnp.where(slot == info[:, k:k + 1], 1.0, 0.0).astype(BF16) for k in range(2)]
        weigh = [info[:, 2 + 3 * k:3 + 3 * k] + info[:, 3 + 3 * k:4 + 3 * k] + info[:, 4 + 3 * k:5 + 3 * k] for k in range(2)]

        def cols(i, carry):
            c = pl.ds(pl.multiple_of(i * tile, tile), tile)
            got = r_in[d, :, c]
            mixed = weigh[0] * jnp.dot(picks[0], got, preferred_element_type=F32)
            mixed += weigh[1] * jnp.dot(picks[1], got, preferred_element_type=F32)
            if d == 0:
                h_in[0, :, c] = mixed.astype(BF16)
            else:
                m_out[d, :, c] = mixed.astype(BF16)
            return carry

        lax.fori_loop(0, feat // tile, cols, 0)
        if d:
            h_copies[d] = remote(m_out.at[d], h_in.at[d], hs.at[d], hr.at[d], at(d, 0))
            h_copies[d].start()

    a, b, c = ORDER
    dispatch(0)
    compute(0)
    dispatch(a)
    combine(0)
    compute(a)
    dispatch(b)
    combine(a)
    compute(b)
    dispatch(c)
    combine(b)
    compute(c)
    combine(c)

    local_group = (tok_group ^ group).astype(F32)
    slot = lax.broadcasted_iota(jnp.int32, (rows, block), 1).astype(F32)
    homes = [
        jnp.where((slot == place) & (local_group == float(d)), 1.0, 0.0).astype(BF16)
        for d in range(GROUPS)
    ]
    for d in ORDER:
        h_copies[d].wait_recv()

    def finish(i, carry):
        c = pl.ds(pl.multiple_of(i * tile, tile), tile)
        total = jnp.dot(homes[0], h_in[0, :, c], preferred_element_type=F32)
        for d in range(1, GROUPS):
            total += jnp.dot(homes[d], h_in[d, :, c], preferred_element_type=F32)
        out[:, c] = total.astype(BF16)
        return carry

    lax.fori_loop(0, feat // tile, finish, 0)
    for copies in (x_copies, y_copies, r_copies, h_copies):
        for copy in copies.values():
            copy.wait_send()


def shards(tokens, norm_gain, route_ids, route_slots, route_weights, w_gate, w_up, w_down):
    rows, feat = tokens.shape
    n_devices = lax.axis_size("ep")
    top_count = route_ids.shape[1]
    cap = 3 * top_count * rows // (2 * n_devices)
    capp = -(-cap // 16) * 16
    peers = n_devices // GROUPS
    block = peers * cap // top_count
    spread = peers * capp
    ffn = w_gate.shape[2]
    vmem = pl.BlockSpec(memory_space=pltpu.VMEM)
    anywhere = pl.BlockSpec(memory_space=pl.ANY)
    dma = pltpu.SemaphoreType.DMA
    return pl.pallas_call(
        functools.partial(kernel, peers, cap, capp),
        out_shape=jax.ShapeDtypeStruct((rows, feat), BF16),
        in_specs=[vmem] * 5 + [anywhere] * 3,
        out_specs=vmem,
        scratch_shapes=[
            pltpu.VMEM((rows, feat + META), BF16),
            pltpu.VMEM((GROUPS, block, feat + META), BF16),
            pltpu.VMEM((GROUPS, block, feat + META), BF16),
            pltpu.VMEM((GROUPS, spread, feat), BF16),
            pltpu.VMEM((GROUPS, spread, feat), BF16),
            pltpu.VMEM((spread, ffn), BF16),
            pltpu.VMEM((GROUPS, spread, feat), BF16),
            pltpu.VMEM((GROUPS, spread, feat), BF16),
            pltpu.VMEM((GROUPS, block, feat), BF16),
            pltpu.VMEM((GROUPS, block, feat), BF16),
            pltpu.VMEM((feat, ffn), BF16),
            pltpu.VMEM((feat, ffn), BF16),
            pltpu.VMEM((ffn, feat), BF16),
            dma((3,)),
            dma((GROUPS,)), dma((GROUPS,)),
            dma((GROUPS, peers)), dma((GROUPS, peers)),
            dma((GROUPS, peers)), dma((GROUPS, peers)),
            dma((GROUPS,)), dma((GROUPS,)),
        ],
        compiler_params=pltpu.CompilerParams(
            collective_id=0, has_side_effects=True, vmem_limit_bytes=60 * 1024 * 1024
        ),
    )(
        tokens, norm_gain.reshape(1, feat), route_ids, route_slots, route_weights,
        w_gate.reshape(feat, ffn), w_up.reshape(feat, ffn), w_down.reshape(ffn, feat),
    )


def solution(mesh):
    placed = (
        P(("grp", "ep"), None),
        P(),
        P(("grp", "ep"), None),
        P(("grp", "ep"), None),
        P(("grp", "ep"), None),
        P("ep", None, None),
        P("ep", None, None),
        P("ep", None, None),
    )
    return jax.shard_map(
        shards, mesh=mesh, in_specs=placed, out_specs=P(("grp", "ep"), None), check_vma=False
    )
```

time: 206 us -> 124 us (0.60)
  Pallas kernels: 0 us -> 116 us
  blocking collectives: 76.4 us -> 0 us
  waiting for transfers between devices: 69.8 us -> 0 us
  local copies, waits for them, and re-layouts: 28.6 us -> 6.72 us
  other arithmetic: 13.8 us -> 0 us
  matrix products: 11.1 us -> 0 us
  starting transfers between devices: 5.24 us -> 0 us
    pallas_call x0 -> x1, Pallas kernels: none -> 116 us  [shards(): pl.pallas_call(functools.partial(kernel, peers, cap, capp), out_shape=jax...]
    all_to_all x1 -> x0, blocking collectives: 76.4 us -> none  [shards(): lax.all_to_all(send, 'ep', split_axis=0, concat_axis=0, tiled=True)]
    all_to_all x1 -> x0, waiting for transfers between devices: 69.8 us -> none  [shards(): lax.all_to_all(results, 'ep', split_axis=0, concat_axis=0, tiled=True)]
    reduce_sum x2 -> x0, other arithmetic: 11.4 us -> none  [the longest x1 9.86 us: shards(): mixed = jnp.sum(route_weights[:, :, None] * picked, axis=1)]
    dot_general x2 -> x0, matrix products: 11.1 us -> none  [the longest x1 8.14 us: shards(): jnp.einsum('sxcf,xfd->sxcd', hidden, w_down, preferred_element_type=jnp.f...]
    gather x1 -> x0, local copies, waits for them, and re-layouts: 7.58 us -> none  [shards(): flat_rows[place_idx].reshape(tok_rows, top_count, feat_dim)]
    scatter x1 -> x0, local copies, waits for them, and re-layouts: 6.73 us -> none  [shards(): send = send.at[place_idx].set(jnp.repeat(normed, top_count, axis=0))]
    convert_element_type x1 -> x0, local copies, waits for them, and re-layouts: 5.48 us -> none  [shards(): flat_rows[place_idx].reshape(tok_rows, top_count, feat_dim)]
  transfers between devices with their start and end apart: 1 -> 0, of which waited for: 1 -> 0; matrix products, arithmetic and copies ran while one was open for 0% -> 0% of each run, Pallas kernels for 0% -> 0%
where the time goes in v1:
time: 124 us; the launch traced here: 123 us
  Pallas kernels  116 us (94%)
  local copies, waits for them, and re-layouts  6.72 us (5%)
    pallas_call x1, Pallas kernels, shards(): pl.pallas_call(functools.partial(kernel, peers, cap, capp), out_shape=jax...  116 us
    unnamed x4, local copies, waits for them, and re-layouts  6.72 us

profile of v1, /device:TPU:15, one launch (start us, length us, event | category | flops | bytes accessed | tf_op | source)
XLA Modules:
  0.0 122.6 jit_solution(15159949392621081313)
XLA Ops:
  0.0 1.5 %copy.9.ids = s32[256,2]{1,0:T(8,128)} copy(s32[256,2]{0,1:T(2,128)} %param.10) | data formatting | bytes 4096 | tf_op args[2]
  1.5 1.5 %copy.10.slots = s32[256,2]{1,0:T(8,128)} copy(s32[256,2]{0,1:T(2,128)} %param.11) | data formatting | bytes 4096 | tf_op args[3]
  2.9 1.5 %copy.11.wts = f32[256,2]{1,0:T(8,128)} copy(f32[256,2]{0,1:T(2,128)} %param.12) | data formatting | bytes 4096 | tf_op args[4]
  4.4 115.9 %shard_map.82 = bf16[256,2048]{1,0:T(8,128)(2,1)} custom-call(bf16[256,2048]{1,0:T(8,128)(2,1)} %tok.1, f32[1,2048]{1,0:T(1,128)} %bitcast.7, s32[256,2]{1,0:T(8,128)} %copy.9.ids, s32[256,2]{1,0:T(8,128)} %copy.10.slots, f32[256,2]{1,0:T(8,128)} %copy.11.wts, bf16[2048,512]{1,0:T(8,128)(2,1)} %bitcast.4, bf16[2048,512]{1,0:T(8,128)(2,1)} %bitcast.5, ...), custom_call_target="tpu_custom_call" | custom-call | tf_op jit(solution)/shard_map/pallas_call | solution.py:259
  120.3 2.3 %copy.13 = bf16[256,2048]{1,0:T(8,128)(2,1)} copy(bf16[256,2048]{1,0:T(8,128)(2,1)} %shard_map.82) | data formatting | bytes 2097152

commit v2 on v0

v2 whole, which is shorter than its diff:
```python
import functools

import jax
import jax.numpy as jnp
from jax import lax
from jax.experimental import pallas as pl
from jax.experimental.pallas import tpu as pltpu
from jax.sharding import PartitionSpec as P

GROUPS = 4
META = 128
CHUNKS = 4
SCHEDULE = (
    "P2", "P0", "D0", "P1", "P3", "H0", "H1", "H2", "H3", "C0", "D2", "D1", "C2", "D3", "M2", "C3", "C1", "M3", "M1", "M0",
)
NT = (((1,), (1,)), ((), ()))
F32 = jnp.float32
BF16 = jnp.bfloat16


def flip(index, bits):
    out, weight = index, 1
    while weight <= bits:
        if bits & weight:
            out = out + weight * (1 - 2 * ((index // weight) % 2))
        weight *= 2
    return out


def where01(hit):
    return jnp.where(hit, 1.0, 0.0).astype(BF16)


def iota(shape, dim):
    return lax.broadcasted_iota(jnp.int32, shape, dim)


def dot(a, b):
    return jnp.dot(a, b, preferred_element_type=F32)


def dot_nt(a, b):
    return lax.dot_general(a, b, NT, preferred_element_type=F32)


def kernel(
    peers, capp,
    tok, gain, ids, slots, wts, wg_hbm, wu_hbm, wd_hbm,
    out,
    normed, meta, n_out, n_in, spreads, picks, homes,
    x_out, x_in, y_out, e_in, hid, r_out, r_in, m_out, h_in, wg, wu, wd,
    w_sem, ns, nr, xs, xr, ys, yr, rs, rr, hs, hr,
):
    rows, feat = tok.shape
    ffn = wg.shape[1]
    block, width = x_out.shape[2:]
    chunks = feat // width
    spread = peers * capp
    me = lax.axis_index("ep")
    group, rank = me // peers, me % peers
    shift = peers.bit_length() - 1
    mesh_id = pl.DeviceIdType.MESH

    def at(d, j):
        return {"ep": flip(group, d) * peers + flip(rank, j)}

    barrier = pltpu.get_barrier_semaphore()
    for d in range(1, GROUPS):
        pl.semaphore_signal(barrier, inc=1, device_id=at(d, 0), device_id_type=mesh_id)
    for j in range(1, peers):
        pl.semaphore_signal(barrier, inc=1, device_id=at(0, j), device_id_type=mesh_id)

    loads = [
        pltpu.make_async_copy(src, dst, w_sem.at[i])
        for i, (src, dst) in enumerate(((wg_hbm, wg), (wu_hbm, wu), (wd_hbm, wd)))
    ]
    for load in loads:
        load.start()

    started = {}

    def send(key, src, dst, sent, got, where):
        copy = pltpu.make_async_remote_copy(
            src_ref=src, dst_ref=dst, send_sem=sent, recv_sem=got,
            device_id=where, device_id_type=mesh_id,
        )
        copy.start()
        started[key] = copy

    step = 32

    def norm_rows(i, carry):
        at_rows = pl.ds(pl.multiple_of(i * step, step), step)
        v = tok[at_rows, :].astype(F32)
        scale = lax.rsqrt(jnp.mean(v * v, axis=-1, keepdims=True) + 1e-06)
        normed[at_rows, :] = (v * scale * gain[...]).astype(BF16)
        return carry

    lax.fori_loop(0, rows // step, norm_rows, 0)

    tok_group = ids[0:1, :] >> shift
    member = where01(iota((16, rows), 0) == tok_group)
    before = dot(member, where01(iota((rows, rows), 0) < iota((rows, rows), 1)))
    place = jnp.sum(before * member.astype(F32), axis=0, keepdims=True)
    kind = iota((META, rows), 0)
    facts = jnp.where(kind == 8, tok_group.astype(F32), jnp.where(kind == 9, place, 0.0))
    for k in range(2):
        code = ((ids[k:k + 1, :] & (peers - 1)) ^ rank) * capp + slots[k:k + 1, :] + 1
        facts = jnp.where(kind == k, code.astype(F32), facts)
        w = wts[k:k + 1, :]
        for part in range(3):
            piece = w.astype(BF16).astype(F32)
            facts = jnp.where(kind == 2 + 3 * k + part, piece, facts)
            w = w - piece
    columns = dot_nt(where01(iota((rows, rows), 0) == iota((rows, rows), 1)), facts.astype(BF16))
    meta[...] = columns.astype(BF16)

    row_no = iota((block, rows), 0).astype(F32)
    tile = min(512, width)

    def tiles(width_of, body):
        def one(i, carry):
            body(pl.multiple_of(i * tile, tile))
            return carry

        lax.fori_loop(0, width_of // tile, one, 0)

    def pack(d):
        chosen = where01((row_no == place) & (tok_group == flip(group, d)))
        n_out[d] = dot(chosen, meta[...]).astype(BF16)
        if d:
            if len(started) == 0:
                pl.semaphore_wait(barrier, GROUPS - 1 + peers - 1)
            send(("n", d), n_out.at[d], n_in.at[d], ns.at[d], nr.at[d], at(d, 0))
        for c in range(chunks):
            def cols(t):
                x_out[d, c, :, pl.ds(t, tile)] = dot(chosen, normed[:, pl.ds(c * width + t, tile)]).astype(BF16)

            tiles(width, cols)
            if d:
                send(("x", d, c), x_out.at[d, c], x_in.at[d, c], xs.at[d, c], xr.at[d, c], at(d, 0))

    def part(j):
        return pl.ds(j * capp, capp)

    far_first = list(range(2, peers)) + [1]

    def dispatch(d):
        src, info = (x_in, n_in) if d else (x_out, n_out)
        if d:
            started["n", d].wait_recv()
        codes = dot_nt(where01(iota((16, META), 0) == iota((16, META), 1)), info[d])
        slot = (iota((spread, block), 0) + 1).astype(F32)
        spreads[d] = where01((slot == codes[0:1, :]) | (slot == codes[1:2, :]))
        for c in range(chunks):
            if d:
                started["x", d, c].wait_recv()

            def cols(t):
                got = dot(spreads[d], src[d, c, :, pl.ds(t, tile)]).astype(BF16)
                e_in[d, c, :capp, pl.ds(t, tile)] = got[:capp]
                y_out[d, c, capp:, pl.ds(t, tile)] = got[capp:]

            tiles(width, cols)
            for j in far_first:
                send(("y", d, c, j), y_out.at[d, c, part(j)], e_in.at[d, c, part(j)],
                     ys.at[d, c, j], yr.at[d, c, j], at(0, j))
        slot = (iota((block, spread), 1) + 1).astype(F32)
        about = info[d].astype(F32)
        for k in range(2):
            picks[d, k] = where01(slot == about[:, k:k + 1])

    def compute(d):
        if loads:
            for load in loads:
                load.wait()
            loads.clear()
        half = 256
        for c in range(chunks):
            for j in range(1, peers):
                started["y", d, c, j].wait_recv()

        def up(i, carry):
            f = pl.ds(pl.multiple_of(i * half, half), half)
            gate = sum(dot(e_in[d, c], wg[c * width:(c + 1) * width, f]) for c in range(chunks))
            upper = sum(dot(e_in[d, c], wu[c * width:(c + 1) * width, f]) for c in range(chunks))
            hid[:, f] = (gate / (1.0 + jnp.exp(-gate)) * upper).astype(BF16)
            return carry

        lax.fori_loop(0, ffn // half, up, 0)
        for c in range(chunks):
            def down(t):
                got = dot(hid[...], wd[:, pl.ds(c * width + t, tile)]).astype(BF16)
                r_in[d, c, :capp, pl.ds(t, tile)] = got[:capp]
                r_out[d, c, capp:, pl.ds(t, tile)] = got[capp:]

            tiles(width, down)
            for j in far_first:
                send(("r", d, c, j), r_out.at[d, c, part(j)], r_in.at[d, c, part(j)],
                     rs.at[d, c, j], rr.at[d, c, j], at(0, j))

    def combine(d):
        info = (n_in if d else n_out)[d].astype(F32)
        weigh = [info[:, b:b + 1] + info[:, b + 1:b + 2] + info[:, b + 2:b + 3] for b in (2, 5)]
        dst = m_out if d else h_in
        for c in range(chunks):
            for j in range(1, peers):
                started["r", d, c, j].wait_recv()

            def cols(t):
                got = r_in[d, c, :, pl.ds(t, tile)]
                mixed = weigh[0] * dot(picks[d, 0], got) + weigh[1] * dot(picks[d, 1], got)
                dst[d, c, :, pl.ds(t, tile)] = mixed.astype(BF16)

            tiles(width, cols)
            if d:
                send(("h", d, c), m_out.at[d, c], h_in.at[d, c], hs.at[d, c], hr.at[d, c], at(d, 0))

    def aim(d):
        slot = iota((rows, block), 1).astype(F32)
        homes[d] = where01((slot == columns[:, 9:10]) & (columns[:, 8:9] == flip(group, d).astype(F32)))

    stages = {"P": pack, "D": dispatch, "C": compute, "M": combine, "H": aim}
    for item in SCHEDULE:
        stages[item[0]](int(item[1]))

    for c in range(chunks):
        for d in range(1, GROUPS):
            started["h", d, c].wait_recv()

        def finish(t):
            total = dot(homes[0], h_in[0, c, :, pl.ds(t, tile)])
            for d in range(1, GROUPS):
                total += dot(homes[d], h_in[d, c, :, pl.ds(t, tile)])
            out[:, pl.ds(c * width + t, tile)] = total.astype(BF16)

        tiles(width, finish)
    for copy in started.values():
        copy.wait_send()


def shards(tokens, norm_gain, route_ids, route_slots, route_weights, w_gate, w_up, w_down):
    rows, feat = tokens.shape
    n_devices = lax.axis_size("ep")
    top_count = route_ids.shape[1]
    cap = 3 * top_count * rows // (2 * n_devices)
    capp = -(-cap // 16) * 16
    peers = n_devices // GROUPS
    block = peers * cap // top_count
    spread = peers * capp
    ffn = w_gate.shape[2]
    width = feat // CHUNKS
    vmem = pl.BlockSpec(memory_space=pltpu.VMEM)
    anywhere = pl.BlockSpec(memory_space=pl.ANY)
    dma = pltpu.SemaphoreType.DMA

    def buf(*shape):
        return pltpu.VMEM(shape, BF16)

    return pl.pallas_call(
        functools.partial(kernel, peers, capp),
        out_shape=jax.ShapeDtypeStruct((rows, feat), BF16),
        in_specs=[vmem] * 5 + [anywhere] * 3,
        out_specs=vmem,
        scratch_shapes=[
            buf(rows, feat), buf(rows, META),
            buf(GROUPS, block, META), buf(GROUPS, block, META),
            buf(GROUPS, spread, block), buf(GROUPS, 2, block, spread), buf(GROUPS, rows, block),
            buf(GROUPS, CHUNKS, block, width), buf(GROUPS, CHUNKS, block, width),
            buf(GROUPS, CHUNKS, spread, width), buf(GROUPS, CHUNKS, spread, width),
            buf(spread, ffn),
            buf(GROUPS, CHUNKS, spread, width), buf(GROUPS, CHUNKS, spread, width),
            buf(GROUPS, CHUNKS, block, width), buf(GROUPS, CHUNKS, block, width),
            buf(feat, ffn), buf(feat, ffn), buf(ffn, feat),
            dma((3,)),
            dma((GROUPS,)), dma((GROUPS,)),
            dma((GROUPS, CHUNKS)), dma((GROUPS, CHUNKS)),
            dma((GROUPS, CHUNKS, peers)), dma((GROUPS, CHUNKS, peers)),
            dma((GROUPS, CHUNKS, peers)), dma((GROUPS, CHUNKS, peers)),
            dma((GROUPS, CHUNKS)), dma((GROUPS, CHUNKS)),
        ],
        compiler_params=pltpu.CompilerParams(
            collective_id=0, has_side_effects=True, vmem_limit_bytes=60 * 1024 * 1024
        ),
    )(
        tokens, norm_gain.reshape(1, feat), route_ids.T, route_slots.T, route_weights.T,
        w_gate.reshape(feat, ffn), w_up.reshape(feat, ffn), w_down.reshape(ffn, feat),
    )


def solution(mesh):
    placed = (
        P(("grp", "ep"), None),
        P(),
        P(("grp", "ep"), None),
        P(("grp", "ep"), None),
        P(("grp", "ep"), None),
        P("ep", None, None),
        P("ep", None, None),
        P("ep", None, None),
    )
    return jax.shard_map(
        shards, mesh=mesh, in_specs=placed, out_specs=P(("grp", "ep"), None), check_vma=False
    )
```

time: 206 us -> 96.1 us (0.47)
  the two profiles are of different devices: /device:TPU:15 before, /device:TPU:0 now
where the time goes in v2:
time: 96.1 us; the launch traced here: 95.9 us
  Pallas kernels  93.6 us (97%)
  local copies, waits for them, and re-layouts  2.3 us (2%)
    pallas_call x1, Pallas kernels, shards(): pl.pallas_call(functools.partial(kernel, peers, capp), out_shape=jax.Shap...  93.6 us
    unnamed x1, local copies, waits for them, and re-layouts  2.3 us

profile of v2, /device:TPU:0, one launch (start us, length us, event | category | flops | bytes accessed | tf_op | source)
XLA Modules:
  0.0 95.9 jit_solution(6836609808366623453)
XLA Ops:
  0.0 93.6 %shard_map.82 = bf16[256,2048]{1,0:T(8,128)(2,1)} custom-call(bf16[256,2048]{1,0:T(8,128)(2,1)} %tok.1, f32[1,2048]{1,0:T(1,128)} %bitcast.10, s32[2,256]{1,0:T(2,128)} %bitcast.11, s32[2,256]{1,0:T(2,128)} %bitcast.12, f32[2,256]{1,0:T(2,128)} %bitcast.13, bf16[2048,512]{1,0:T(8,128)(2,1)} %bitcast.7, bf16[2048,512]{1,0:T(8,128)(2,1)} %bitcast.8, ...), custom_call_target="tpu_custom_call" | custom-call | tf_op jit(solution)/shard_map/pallas_call | solution.py:260
  93.6 2.3 %copy.10 = bf16[256,2048]{1,0:T(8,128)(2,1)} copy(bf16[256,2048]{1,0:T(8,128)(2,1)} %shard_map.82) | data formatting | bytes 2097152
